TPU v7x, 32 devices: a whole 2x2x4 slice. The times are simulated.
32 devices in a mesh: ep: 16 (over z, y, x), tp: 2 (over core).
Axes of the slice: x: 2, y: 2, z: 4, core: 2. Of those that a mesh axis runs over, the one named last changes fastest.
Arguments:
- tokens: bfloat16 [256, 2048], P('ep'), may hold values from -6 to 6
- norm_gain: bfloat16 [2048], replicated, may hold values from 0.099609375 to 1.8984375
- w_query: bfloat16 [2048, 512], P(None, 'tp'), may hold values from -0.125 to 0.125
- w_key: bfloat16 [2048, 256], P(None, 'tp'), may hold values from -0.125 to 0.125
- w_value: bfloat16 [2048, 256], P(None, 'tp'), may hold values from -0.125 to 0.125
- w_forget: bfloat16 [2048, 8], P(None, 'tp'), may hold values from -0.25 to 0.25
- w_out: bfloat16 [512, 2048], P('tp'), may hold values from -0.25 to 0.25
- cache_keys: bfloat16 [256, 1024, 256], P('ep', None, 'tp'), may hold values from -700 to 700
- cache_values: bfloat16 [256, 1024, 256], P('ep', None, 'tp'), may hold values from -6 to 6
- cache_gates: float32 [256, 8, 1024], P('ep', 'tp'), as said below
- lengths: int32 [256], P('ep'), may hold values from 1 to 1024, as said below
- ffn_gain: bfloat16 [2048], replicated, may hold values from 0.099609375 to 1.8984375
- router_w: bfloat16 [2048, 16], replicated, may hold values from -0.125 to 0.125
- routes: int32 [256, 6], P('ep'), may hold values from 0 to 15, all different within a row; in each aligned block of 16 rows (0 to 15, 16 to 31, ...) at most 12 rows name the same one
- shared_gate: bfloat16 [2048, 512], P(None, 'tp'), may hold values from -0.125 to 0.125
- shared_up: bfloat16 [2048, 512], P(None, 'tp'), may hold values from -0.125 to 0.125
- shared_down: bfloat16 [512, 2048], P('tp'), may hold values from -0.25 to 0.25
- expert_gate: bfloat16 [16, 2048, 512], P('ep', None, 'tp'), may hold values from -0.125 to 0.125
- expert_up: bfloat16 [16, 2048, 512], P('ep', None, 'tp'), may hold values from -0.125 to 0.125
- expert_down: bfloat16 [16, 512, 2048], P('ep', 'tp'), may hold values from -0.25 to 0.25
Outputs:
- layer_out: bfloat16 [256, 2048], P('ep')
Inputs may be any that keep to these rules, and one draw needn't show every extreme that they name: `routes`: each row names 6 different experts. Among the rows of one index of ep no expert is named by more than 12 rows, and in every draw some expert is named by exactly 12 of them. `lengths`: in every draw some sequence has all 1024 positions. `cache_gates`: each row is non-increasing along the positions.
All inputs are finite; a program needn't handle non-finite values.
Results may differ from a plain program's by a relative error of at most 0.017.
Values may be sent and summed in bfloat16 or wider, within the bound.
A program may use at most 64 MiB of HBM per device.

v0:
```python
import jax
import jax.numpy as jnp
from jax import lax
from jax.sharding import PartitionSpec as P

HEAD_DIM = 64


EPS = 1e-06
ROUTE_SCALE = 2.5


def norm_rows(rows, norm_gain):
    values = rows.astype(jnp.float32)
    factor = lax.rsqrt(jnp.mean(values * values, axis=-1, keepdims=True) + EPS)
    return (values * factor * norm_gain.astype(jnp.float32)).astype(jnp.bfloat16)


def swiglu_hidden(rows, w_gate, w_up):
    gate_proj = jnp.dot(rows, w_gate, preferred_element_type=jnp.float32)
    upward = jnp.dot(rows, w_up, preferred_element_type=jnp.float32)
    return (jax.nn.silu(gate_proj) * upward).astype(jnp.bfloat16)


def route_weights(rows, router_w, chosen):
    scores = jax.nn.sigmoid(jnp.dot(rows, router_w, preferred_element_type=jnp.float32))
    picked = jnp.take_along_axis(scores, chosen, axis=1)
    return ROUTE_SCALE * picked / jnp.sum(picked, axis=1, keepdims=True)


def slot_hidden(incoming, expert_gate, expert_up):
    gate_proj = jnp.einsum(
        "scd,df->scf", incoming, expert_gate[0], preferred_element_type=jnp.float32
    )
    upward = jnp.einsum("scd,df->scf", incoming, expert_up[0], preferred_element_type=jnp.float32)
    return (jax.nn.silu(gate_proj) * upward).astype(jnp.bfloat16)


def attend(
    normed, w_query, w_key, w_value, w_forget, cache_keys, cache_values, cache_gates, lengths
):
    seq_count = normed.shape[0]
    head_count = w_forget.shape[1]
    kv_count = w_key.shape[1] // HEAD_DIM
    group_size = head_count // kv_count
    cache_len = cache_keys.shape[1]
    score_scale = HEAD_DIM ** (-0.5)
    queries = jnp.dot(normed, w_query, preferred_element_type=jnp.float32).astype(jnp.bfloat16)
    queries = queries.reshape(seq_count, kv_count, group_size, HEAD_DIM)
    key_new = jnp.dot(normed, w_key, preferred_element_type=jnp.float32).astype(jnp.bfloat16)
    key_new = key_new.reshape(seq_count, kv_count, HEAD_DIM)
    value_new = jnp.dot(normed, w_value, preferred_element_type=jnp.float32).astype(jnp.bfloat16)
    value_new = value_new.reshape(seq_count, kv_count, HEAD_DIM)
    log_gate = jax.nn.log_sigmoid(jnp.dot(normed, w_forget, preferred_element_type=jnp.float32))
    cached_keys = cache_keys.reshape(seq_count, cache_len, kv_count, HEAD_DIM)
    cached_values = cache_values.reshape(seq_count, cache_len, kv_count, HEAD_DIM)
    past_score = (
        jnp.einsum("skgd,slkd->skgl", queries, cached_keys, preferred_element_type=jnp.float32)
        * score_scale
    )
    last_index = jnp.broadcast_to((lengths - 1)[:, None, None], (seq_count, head_count, 1))
    last_gate = jnp.take_along_axis(cache_gates, last_index, axis=2)
    gate_bias = last_gate + log_gate[:, :, None] - cache_gates
    past_score = past_score + gate_bias.reshape(seq_count, kv_count, group_size, cache_len)
    is_valid = jnp.arange(cache_len)[None, :] < lengths[:, None]
    past_score = jnp.where(is_valid[:, None, None, :], past_score, -jnp.inf)
    self_score = (
        jnp.einsum("skgd,skd->skg", queries, key_new, preferred_element_type=jnp.float32)
        * score_scale
    )
    peak_score = jnp.maximum(jnp.max(past_score, axis=-1), self_score)
    past_weight = jnp.exp(past_score - peak_score[..., None])
    self_weight = jnp.exp(self_score - peak_score)
    weight_sum = jnp.sum(past_weight, axis=-1) + self_weight
    past_prob = (past_weight / weight_sum[..., None]).astype(jnp.bfloat16)
    self_prob = (self_weight / weight_sum).astype(jnp.bfloat16)
    mixed_heads = jnp.einsum(
        "skgl,slkd->skgd", past_prob, cached_values, preferred_element_type=jnp.float32
    )
    mixed_heads = (
        mixed_heads
        + self_prob.astype(jnp.float32)[..., None] * value_new.astype(jnp.float32)[:, :, None, :]
    )
    return mixed_heads.astype(jnp.bfloat16).reshape(seq_count, head_count * HEAD_DIM)


def per_device(
    tokens,
    norm_gain,
    w_query,
    w_key,
    w_value,
    w_forget,
    w_out,
    cache_keys,
    cache_values,
    cache_gates,
    lengths,
    ffn_gain,
    router_w,
    routes,
    shared_gate,
    shared_up,
    shared_down,
    expert_gate,
    expert_up,
    expert_down,
):
    seq_count = tokens.shape[0]
    width = tokens.shape[1]
    top_k = routes.shape[1]
    groups = lax.axis_size("ep")
    capacity = max(2, 2 * seq_count * top_k // groups)
    normed = norm_rows(tokens, norm_gain)
    attn = attend(
        normed, w_query, w_key, w_value, w_forget, cache_keys, cache_values, cache_gates, lengths
    )
    partial_value = jnp.dot(attn, w_out, preferred_element_type=jnp.float32)
    attended = lax.psum(partial_value.astype(jnp.bfloat16), "tp").astype(jnp.float32)
    residual_rows = (tokens.astype(jnp.float32) + attended).astype(jnp.bfloat16)
    ffn_rows = norm_rows(residual_rows, ffn_gain)
    shared_part = jnp.dot(
        swiglu_hidden(ffn_rows, shared_gate, shared_up),
        shared_down,
        preferred_element_type=jnp.float32,
    )
    flat_routes = routes.reshape(-1)
    expert_marks = (flat_routes[:, None] == jnp.arange(groups, dtype=jnp.int32)[None, :]).astype(
        jnp.int32
    )
    before = jnp.cumsum(expert_marks, axis=0) - expert_marks
    slot_rank = jnp.sum(before * expert_marks, axis=1)
    target = flat_routes * capacity + slot_rank
    sources = jnp.repeat(ffn_rows, top_k, axis=0)
    outgoing = jnp.zeros((groups * capacity, width), jnp.bfloat16).at[target].set(sources)
    outgoing = outgoing.reshape(groups, capacity, width)
    weights = route_weights(ffn_rows, router_w, routes)
    shared = lax.psum(shared_part.astype(jnp.bfloat16), "tp").astype(jnp.float32)
    hidden = slot_hidden(
        lax.all_to_all(outgoing, "ep", split_axis=0, concat_axis=0, tiled=True),
        expert_gate,
        expert_up,
    )
    part_rows = jnp.einsum(
        "scf,fd->scd", hidden, expert_down[0], preferred_element_type=jnp.float32
    )
    merged = lax.psum(part_rows.astype(jnp.bfloat16), "tp")
    returned = lax.all_to_all(merged, "ep", split_axis=0, concat_axis=0, tiled=True)
    answers = returned.reshape(groups * capacity, width)[target].astype(jnp.float32)
    routed = jnp.sum((answers * weights.reshape(-1, 1)).reshape(seq_count, top_k, width), axis=1)
    return (residual_rows.astype(jnp.float32) + shared + routed).astype(jnp.bfloat16)


def solution(mesh):
    placed = (
        P("ep", None),
        P(),
        P(None, "tp"),
        P(None, "tp"),
        P(None, "tp"),
        P(None, "tp"),
        P("tp", None),
        P("ep", None, "tp"),
        P("ep", None, "tp"),
        P("ep", "tp", None),
        P("ep"),
        P(),
        P(),
        P("ep", None),
        P(None, "tp"),
        P(None, "tp"),
        P("tp", None),
        P("ep", None, "tp"),
        P("ep", None, "tp"),
        P("ep", "tp", None),
    )
    return jax.shard_map(
        per_device, mesh=mesh, in_specs=placed, out_specs=P("ep", None), check_vma=False
    )
```

profile of v0, /device:TPU:29, one launch (start us, length us, event | category | flops | bytes accessed | tf_op | source)
XLA Modules:
  0.0 156.8 jit_solution(10485260314686976867)
XLA Ops:
  6.5 0.7 broadcast_add_fusion
  7.3 0.7 broadcast_compare_fusion
  7.9 0.7 iota_compare_fusion
  8.8 0.1 reshape.274
  9.0 2.0 %gather_fusion.1 = f32[64]{0:T(128)S(1)} fusion(f32[16,4,1024]{2,1,0:T(4,128)} %param.29, s32[64]{0:T(128)S(1)} %reshape.274), kind=kCustom, calls=%fused_computation.1 | custom fusion | bytes 1280 | tf_op jit(solution)/shard_map/jit(take_along_axis)/gather | solution.py:62
  11.2 0.1 fusion.17
  11.4 0.2 fusion.39
  11.7 0.1 broadcast_subtract_fusion
  11.8 0.2 reshape.254
  12.0 0.3 convolution_convert_fusion.3
  12.3 0.1 reshape.252
  12.4 6.5 %copy.41 = bf16[16,1024,128]{1,2,0:T(8,128)(2,1)} copy(bf16[16,1024,128]{2,1,0:T(8,128)(2,1)} %param.27) | data formatting | bytes 8388608 | tf_op args[7]
  18.9 0.2 convolution_convert_fusion.5
  19.2 0.2 fusion.56
  19.4 3.0 %fusion.55 = (f32[16,2,2]{2,1,0:T(2,128)S(1)}, f32[16,2,2,1024]{3,2,1,0:T(2,128)S(1)}) fusion(f32[16,2,2,1024]{3,2,1,0:T(2,128)S(1)} %reshape.254, bf16[16,2,2,64]{3,2,1,0:T(2,128)(2,1)S(1)} %reshape.252, bf16[16,1024,2,64]{1,3,2,0:T(8,128)(2,1)} %bitcast.50, pred[16,1024]{1,0:T(8,128)(4,1)S(1)} %iota_compare_fusion), kind=kOutput, calls=%fused_computation.103 | convolution fusion | flops 8650688 | bytes 4743424 | tf_op jit(solution)/shard_map/skgd,slkd->skgl/dot_general | solution.py:58
  22.4 0.3 fusion.16
  22.8 0.2 fusion.7
  23.1 6.4 %copy.45 = bf16[16,1024,128]{1,2,0:T(8,128)(2,1)} copy(bf16[16,1024,128]{2,1,0:T(8,128)(2,1)} %param.28) | data formatting | bytes 8388608 | tf_op args[8]
  29.5 3.5 %fusion.2 = bf16[16,2,2,64]{3,2,1,0:T(2,128)(2,1)S(1)} fusion(bf16[16,1024,2,64]{1,3,2,0:T(8,128)(2,1)} %bitcast.51, f32[16,2,2,1024]{3,2,1,0:T(2,128)S(1)} %get-tuple-element.12, f32[16,2,2]{2,1,0:T(2,128)S(1)} %get-tuple-element.8, f32[16,2,2]{2,1,0:T(2,128)S(1)} %multiply_maximum_fusion, f32[16,2,64]{2,1,0:T(2,128)S(1)} %reshape.262, ...), kind=kOutput, calls=%fused_computation.11 | convolution fusion | flops 8597504 | bytes 4473600 | tf_op jit(solution)/shard_map/skgl,slkd->skgd/dot_general | solution.py:77
  33.0 0.1 reshape.257
  33.1 0.9 convolution_convert_fusion.2
  34.3 0.1 reduce_window_sum.11
  34.4 0.2 select_reduce_fusion
  34.7 0.1 mul.136
  34.8 18.7 %all-reduce.4.cloned.1.call-done = bf16[16,2048]{1,0:T(8,128)(2,1)} async-done(((bf16[16,2048]{1,0:T(8,128)(2,1)}), bf16[16,2048]{1,0:T(8,128)(2,1)}) %all-reduce.4.cloned.1.call-update) | async-done | bytes 65552 | tf_op jit(solution)/shard_map/psum | solution.py:119
  53.6 1.0 fusion.21
  54.5 0.9 fusion.23
  55.5 0.1 reshape.290
  55.7 1.4 scatter_custom_fusion
  57.1 1.2 reshape.259
  58.3 6.4 %all-to-all-start = ((bf16[16,12,2048]{2,1,0:T(8,128)(2,1)}), bf16[16,12,2048]{2,1,0:T(8,128)(2,1)S(1)}, u32[]{:S(2)}, u32[]{:S(2)}) async-start(bf16[16,12,2048]{2,1,0:T(8,128)(2,1)} %reshape.259), calls=%async_computation | async-start | bytes 2097152 | tf_op jit(solution)/shard_map/all_to_all | solution.py:140
  64.7 1.5 fusion.57
  66.2 2.9 %convolution_convert_fusion.1 = bf16[16,2048]{1,0:T(8,128)(2,1)} fusion(bf16[256,2048]{1,0:T(8,128)(2,1)} %param.36, bf16[16,2048]{1,0:T(8,128)(2,1)S(1)} %fusion.23, bf16[2048,256]{1,0:T(8,128)(2,1)} %param.35, f32[16,256]{1,0:T(8,128)S(1)} %fusion.57), kind=kOutput, calls=%fused_computation.5 | convolution fusion | flops 33611776 | bytes 2244608 | tf_op jit(solution)/shard_map/dot_general | solution.py:122
  69.1 19.6 %all-to-all-done = bf16[16,12,2048]{2,1,0:T(8,128)(2,1)S(1)} async-done(((bf16[16,12,2048]{2,1,0:T(8,128)(2,1)}), bf16[16,12,2048]{2,1,0:T(8,128)(2,1)S(1)}, u32[]{:S(2)}, u32[]{:S(2)}) %all-to-all-start) | async-done | bytes 786464 | tf_op jit(solution)/shard_map/all_to_all | solution.py:140
  88.7 1.7 %fusion.11 = f32[16,12,256]{2,1,0:T(8,128)S(1)} fusion(bf16[16,12,2048]{2,1,0:T(8,128)(2,1)S(1)} %all-to-all-done, bf16[1,2048,256]{2,1,0:T(8,128)(2,1)} %param.37), kind=kOutput, calls=%fused_computation.26 | convolution fusion | flops 201326592 | bytes 2031616 | tf_op jit(solution)/shard_map/scd,df->scf/dot_general | solution.py:32
  90.4 1.7 %fusion.9 = f32[16,12,256]{2,1,0:T(8,128)S(1)} fusion(bf16[16,12,2048]{2,1,0:T(8,128)(2,1)S(1)} %all-to-all-done, bf16[1,2048,256]{2,1,0:T(8,128)(2,1)} %param.38), kind=kOutput, calls=%fused_computation.24 | convolution fusion | flops 201326592 | bytes 2031616 | tf_op jit(solution)/shard_map/scd,df->scf/dot_general | solution.py:35
  92.1 1.5 convolution_convert_fusion
  93.6 21.2 %all-reduce.6.cloned.1.call-done = (bf16[16,12,2048]{2,0,1:T(8,128)(2,1)}, bf16[16,2048]{1,0:T(8,128)(2,1)}) async-done(((bf16[16,12,2048]{2,0,1:T(8,128)(2,1)}, bf16[16,2048]{1,0:T(8,128)(2,1)}), (bf16[16,12,2048]{2,0,1:T(8,128)(2,1)}, bf16[16,2048]{1,0:T(8,128)(2,1)})) %all-reduce.6.cloned.1.call-update) | async-done | bytes 851984 | tf_op jit(solution)/shard_map/psum | solution.py:147
  114.8 2.6 %copy.50 = bf16[16,12,2048]{2,1,0:T(8,128)(2,1)} copy(bf16[16,12,2048]{2,0,1:T(8,128)(2,1)} %get-tuple-element.5) | data formatting | bytes 1572864 | tf_op jit(solution)/shard_map/psum | solution.py:147
  117.3 6.4 %all-to-all-start.1 = ((bf16[16,12,2048]{2,1,0:T(8,128)(2,1)}), bf16[16,12,2048]{2,1,0:T(8,128)(2,1)S(1)}, u32[]{:S(2)}, u32[]{:S(2)}) async-start(bf16[16,12,2048]{2,1,0:T(8,128)(2,1)} %copy.50), calls=%async_computation.1 | async-start | bytes 2097152 | tf_op jit(solution)/shard_map/all_to_all | solution.py:148
  123.9 0.1 fusion.6
  124.0 1.3 gather_fusion.2
  125.7 22.1 %all-to-all-done.1 = bf16[16,12,2048]{2,1,0:T(8,128)(2,1)S(1)} async-done(((bf16[16,12,2048]{2,1,0:T(8,128)(2,1)}), bf16[16,12,2048]{2,1,0:T(8,128)(2,1)S(1)}, u32[]{:S(2)}, u32[]{:S(2)}) %all-to-all-start.1) | async-done | bytes 786464 | tf_op jit(solution)/shard_map/all_to_all | solution.py:148
  147.8 0.2 reshape.260
  147.9 0.8 gather_fusion
  148.8 0.1 reshape.263
  148.9 0.4 multiply_reduce_fusion
  149.3 0.7 fusion.25
  (65 shorter events, 1.6 us)
Async XLA Ops:
  6.5 85.5 %copy-start = (bf16[1,256,2048]{2,1,0:T(8,128)(2,1)S(1)}, bf16[1,256,2048]{2,1,0:T(8,128)(2,1)}, u32[]{:S(2)}) copy-start(bf16[1,256,2048]{2,1,0:T(8,128)(2,1)} %param.39) | copy-start | bytes 3145732
  6.5 47.0 %all-reduce.4.cloned.1.call-start = ((), (), s32[]{:S(2)}) async-start(), calls=%async_computation.2 | async-start | bytes 131072 | tf_op jit(solution)/shard_map/psum | solution.py:119
  8.9 2.3 %copy-start.10 = (bf16[2048]{0:T(1024)(128)(2,1)S(1)}, bf16[2048]{0:T(1024)(128)(2,1)}, u32[]{:S(2)}) copy-start(bf16[2048]{0:T(1024)(128)(2,1)} %param.21) | copy-start | bytes 12292
  8.9 2.3 %copy-start.2 = (bf16[16,2048]{1,0:T(8,128)(2,1)S(1)}, bf16[16,2048]{1,0:T(8,128)(2,1)}, u32[]{:S(2)}) copy-start(bf16[16,2048]{1,0:T(8,128)(2,1)} %param.20) | copy-start | bytes 196612
  8.9 2.4 %copy-start.13 = (bf16[2048,4]{0,1:T(4,128)(2,1)S(1)}, bf16[2048,4]{0,1:T(4,128)(2,1)}, u32[]{:S(2)}) copy-start(bf16[2048,4]{0,1:T(4,128)(2,1)} %param.25) | copy-start | bytes 49156
  9.0 2.7 %copy-start.1 = (f32[16,4,1024]{2,1,0:T(4,128)S(1)}, f32[16,4,1024]{2,1,0:T(4,128)}, u32[]{:S(2)}) copy-start(f32[16,4,1024]{2,1,0:T(4,128)} %param.29) | copy-start | bytes 786436
  9.0 3.0 %copy-start.3 = (bf16[2048,256]{1,0:T(8,128)(2,1)S(1)}, bf16[2048,256]{1,0:T(8,128)(2,1)}, u32[]{:S(2)}) copy-start(bf16[2048,256]{1,0:T(8,128)(2,1)} %param.22) | copy-start | bytes 3145732
  12.4 6.5 %copy-start.6 = (bf16[2048,128]{1,0:T(8,128)(2,1)S(1)}, bf16[2048,128]{1,0:T(8,128)(2,1)}, u32[]{:S(2)}) copy-start(bf16[2048,128]{1,0:T(8,128)(2,1)} %param.23) | copy-start | bytes 1572868
  18.9 3.9 %copy-start.7 = (bf16[2048,128]{1,0:T(8,128)(2,1)S(1)}, bf16[2048,128]{1,0:T(8,128)(2,1)}, u32[]{:S(2)}) copy-start(bf16[2048,128]{1,0:T(8,128)(2,1)} %param.24) | copy-start | bytes 1572868
  29.5 3.6 %copy-start.4 = (bf16[256,2048]{1,0:T(8,128)(2,1)S(1)}, bf16[256,2048]{1,0:T(8,128)(2,1)}, u32[]{:S(2)}) copy-start(bf16[256,2048]{1,0:T(8,128)(2,1)} %param.26) | copy-start | bytes 3145732
  29.5 4.5 %copy-start.8 = (s32[16,6]{0,1:T(8,128)S(1)}, s32[16,6]{0,1:T(8,128)}, u32[]{:S(2)}) copy-start(s32[16,6]{0,1:T(8,128)} %param.33) | copy-start | bytes 1156
  29.5 5.3 %copy-start.11 = (bf16[2048]{0:T(1024)(128)(2,1)S(1)}, bf16[2048]{0:T(1024)(128)(2,1)}, u32[]{:S(2)}) copy-start(bf16[2048]{0:T(1024)(128)(2,1)} %param.31) | copy-start | bytes 12292
  58.3 30.4 %all-to-all-start = ((bf16[16,12,2048]{2,1,0:T(8,128)(2,1)}), bf16[16,12,2048]{2,1,0:T(8,128)(2,1)S(1)}, u32[]{:S(2)}, u32[]{:S(2)}) async-start(bf16[16,12,2048]{2,1,0:T(8,128)(2,1)} %reshape.259), calls=%async_computation | async-start | bytes 2097152 | tf_op jit(solution)/shard_map/all_to_all | solution.py:140
  64.6 50.1 %all-reduce.6.cloned.1.call-start = ((), (), s32[]{:S(2)}) async-start(), calls=%async_computation.3 | async-start | bytes 1703936 | tf_op jit(solution)/shard_map/psum | solution.py:147
  90.4 33.5 %copy-start.12 = (bf16[2048,16]{0,1:T(8,128)(2,1)S(1)}, bf16[2048,16]{0,1:T(8,128)(2,1)}, u32[]{:S(2)}) copy-start(bf16[2048,16]{0,1:T(8,128)(2,1)} %param.32) | copy-start | bytes 196612
  117.3 30.4 %all-to-all-start.1 = ((bf16[16,12,2048]{2,1,0:T(8,128)(2,1)}), bf16[16,12,2048]{2,1,0:T(8,128)(2,1)S(1)}, u32[]{:S(2)}, u32[]{:S(2)}) async-start(bf16[16,12,2048]{2,1,0:T(8,128)(2,1)} %copy.50), calls=%async_computation.1 | async-start | bytes 2097152 | tf_op jit(solution)/shard_map/all_to_all | solution.py:148
  125.3 23.9 %copy-start.5 = (bf16[16,2048]{1,0:T(8,128)(2,1)S(1)}, bf16[16,2048]{1,0:T(8,128)(2,1)}, u32[]{:S(2)}) copy-start(bf16[16,2048]{1,0:T(8,128)(2,1)} %all-reduce.4.cloned.1.call-done) | copy-start | bytes 196612
  125.4 23.9 %copy-start.9 = (bf16[16,2048]{1,0:T(8,128)(2,1)S(1)}, bf16[16,2048]{1,0:T(8,128)(2,1)}, u32[]{:S(2)}) copy-start(bf16[16,2048]{1,0:T(8,128)(2,1)} %get-tuple-element.6) | copy-start | bytes 196612
Sparse Core Ops, SparseCore 0:
  34.1 19.3 all-reduce.3
  93.7 21.0 all-reduce.5
where the time goes:
time: 160 us; the launch traced here: 157 us
  waiting for transfers between devices  81.7 us (51%)
  local copies, waits for them, and re-layouts  24.5 us (15%)
  matrix products  17.9 us (11%)
  between operations  13.8 us (9%)
  starting transfers between devices  12.8 us (8%)
  other arithmetic  6.22 us (4%)
    all_to_all x1, waiting for transfers between devices, per_device(): lax.all_to_all(merged, 'ep', split_axis=0, concat_axis=0, tiled=True)  22.1 us
    psum x1, waiting for transfers between devices, per_device(): merged = lax.psum(part_rows.astype(jnp.bfloat16), 'tp')  21.2 us
    all_to_all x1, waiting for transfers between devices, per_device(): lax.all_to_all(outgoing, 'ep', split_axis=0, concat_axis=0, tiled=True)  19.6 us
    psum x1, waiting for transfers between devices, per_device(): lax.psum(partial_value.astype(jnp.bfloat16), 'tp').astype(jnp.float32)  18.7 us
    unnamed x33, local copies, waits for them, and re-layouts  13 us
    all_to_all x1, starting transfers between devices, per_device(): lax.all_to_all(merged, 'ep', split_axis=0, concat_axis=0, tiled=True)  6.36 us
    all_to_all x1, starting transfers between devices, per_device(): lax.all_to_all(outgoing, 'ep', split_axis=0, concat_axis=0, tiled=True)  6.36 us
    dot_general x1, matrix products, attend(): jnp.einsum('skgl,slkd->skgd', past_prob, cached_values, preferred_element...  3.52 us
  transfers between devices with their start and end apart: 4, of which 4 were waited for; matrix products, arithmetic and copies ran while one was open for 4% of the time, Pallas kernels for 0%

commit v1 on v0

v1 whole, which is shorter than its diff:
```python
import functools

import jax
import jax.numpy as jnp
from jax import lax
from jax.experimental import pallas as pl
from jax.experimental.pallas import tpu as pltpu
from jax.sharding import PartitionSpec as P

HEAD_DIM = 64
EPS = 1e-06
ROUTE_SCALE = 2.5
MESH = pl.DeviceIdType.MESH
F32 = jnp.float32
BF16 = jnp.bfloat16


def dot(a, b):
    return jnp.dot(a, b, preferred_element_type=F32)


def dot_t(a, b):
    return lax.dot_general(a, b, (((1,), (1,)), ((), ())), preferred_element_type=F32)


def norm_rows(values, gain):
    factor = lax.rsqrt(jnp.mean(values * values, axis=-1, keepdims=True) + EPS)
    return (values * factor * gain.astype(F32)).astype(BF16)


def silu(x):
    return x * jax.nn.sigmoid(x)


def attend_kernel(
    len_ref, tok_ref, gain_ref, wq_ref, wk_ref, wv_ref, wf_ref, wo_ref, kc_ref, vc_ref, cg_ref,
    out_ref, qs, lg, ss, vn, ob,
):
    step = pl.program_id(0)
    steps = pl.num_programs(0)
    per_step, positions, kv_width = kc_ref.shape
    seqs = tok_ref.shape[0]
    heads = wf_ref.shape[0]
    kv_count = kv_width // HEAD_DIM
    group = heads // kv_count
    scale = HEAD_DIM ** (-0.5)

    @pl.when(step == 0)
    def _():
        normed = norm_rows(tok_ref[...].astype(F32), gain_ref[...])
        q = dot(normed, wq_ref[...]).astype(BF16).astype(F32)
        kn = dot(normed, wk_ref[...]).astype(BF16).astype(F32)
        vn[...] = dot(normed, wv_ref[...]).astype(BF16).astype(F32)
        fg = dot_t(normed, wf_ref[...])
        log_gate = jnp.minimum(fg, 0.0) - jnp.log1p(jnp.exp(-jnp.abs(fg)))
        lane = lax.broadcasted_iota(jnp.int32, (seqs, kv_width), 1)
        for h in range(heads):
            kv = h // group
            base = (h * HEAD_DIM) // kv_width * kv_width
            blk = q[:, base : base + kv_width]
            shift = (kv * HEAD_DIM - (h * HEAD_DIM - base)) % kv_width
            if shift:
                blk = pltpu.roll(blk, shift, 1)
            blk = jnp.where((lane >= kv * HEAD_DIM) & (lane < (kv + 1) * HEAD_DIM), blk, 0.0)
            qs[:, h, :] = blk
            lg[:, h, :] = jnp.broadcast_to(log_gate[:, h : h + 1], (seqs, 128))
            own = jnp.sum(blk * kn, axis=1, keepdims=True) * scale
            ss[:, h, :] = jnp.broadcast_to(own, (seqs, 128))

    pos = lax.broadcasted_iota(jnp.int32, (heads, positions), 1)
    lane1 = lax.broadcasted_iota(jnp.int32, (1, kv_width), 1)
    for j in range(per_step):
        b = step * per_step + j
        n = len_ref[b]
        score = dot_t(qs[b].astype(BF16), kc_ref[j])
        gates = cg_ref[j]
        last = jnp.sum(jnp.where(pos == n - 1, gates, 0.0), axis=1, keepdims=True)
        score = score * scale + (last + lg[b][:, :1] - gates)
        score = jnp.where(pos < n, score, -jnp.inf)
        own = ss[b][:, :1]
        peak = jnp.maximum(jnp.max(score, axis=1, keepdims=True), own)
        weight = jnp.exp(score - peak)
        own_weight = jnp.exp(own - peak)
        inv = 1.0 / (jnp.sum(weight, axis=1, keepdims=True) + own_weight)
        prob = (weight * inv).astype(BF16)
        own_prob = (own_weight * inv).astype(BF16).astype(F32)
        mixed = dot(prob, vc_ref[j]) + own_prob * vn[pl.ds(b, 1), :]
        for g in range(group):
            row = mixed[g : g + 1]
            for kv in range(1, kv_count):
                row = jnp.where(lane1 >= kv * HEAD_DIM, mixed[kv * group + g : kv * group + g + 1], row)
            ob[g, pl.ds(b, 1), :] = row

    @pl.when(step == steps - 1)
    def _():
        total = jnp.zeros((seqs, wo_ref.shape[1]), F32)
        for g in range(group):
            rows = [
                wo_ref[(kv * group + g) * HEAD_DIM : (kv * group + g + 1) * HEAD_DIM, :]
                for kv in range(kv_count)
            ]
            total = total + dot(ob[g].astype(BF16), jnp.concatenate(rows, axis=0))
        out_ref[...] = total.astype(BF16)


def experts_kernel(
    n, per_chunk, part_ref, tok_ref, gain_ref, router_ref, routes_ref,
    sg_hbm, su_hbm, sd_hbm, eg_hbm, eu_hbm, ed_hbm, out_ref,
    sg, su, sd, eg, eu, ed, other, rows_all, resid, sh_send, sh_recv, sh_keep,
    p_send, p_recv, p_keep, answer, ret, halves, weights,
    wsem, tsend, trecv, dsend, drecv, rsend, rrecv, psend, precv, asend, arecv,
):
    i = lax.axis_index("ep")
    t = lax.axis_index("tp")
    u = 1 - t
    seqs, width = tok_ref.shape
    half = width // 2
    chunks = n // per_chunk
    rows = per_chunk * seqs
    partner = (i, u)

    loads = [
        pltpu.make_async_copy(sg_hbm, sg, wsem.at[0]),
        pltpu.make_async_copy(su_hbm, su, wsem.at[1]),
        pltpu.make_async_copy(sd_hbm.at[:, pl.ds(0, half)], sd.at[0], wsem.at[2]),
        pltpu.make_async_copy(sd_hbm.at[:, pl.ds(half, half)], sd.at[1], wsem.at[3]),
        pltpu.make_async_copy(eg_hbm.at[0], eg, wsem.at[4]),
        pltpu.make_async_copy(eu_hbm.at[0], eu, wsem.at[5]),
        pltpu.make_async_copy(ed_hbm.at[0, :, pl.ds(0, half)], ed.at[0], wsem.at[6]),
        pltpu.make_async_copy(ed_hbm.at[0, :, pl.ds(half, half)], ed.at[1], wsem.at[7]),
    ]
    for load in loads:
        load.start()

    barrier = pltpu.get_barrier_semaphore()
    pl.semaphore_signal(barrier, inc=1, device_id=partner, device_id_type=MESH)

    @pl.loop(1, n)
    def _(k):
        pl.semaphore_signal(barrier, inc=1, device_id=(lax.rem(i + k, n), t), device_id_type=MESH)

    pl.semaphore_wait(barrier, n)

    def remote(src, dst, ssem, rsem, dev):
        return pltpu.make_async_remote_copy(
            src_ref=src, dst_ref=dst, send_sem=ssem, recv_sem=rsem, device_id=dev,
            device_id_type=MESH,
        )

    swap = remote(part_ref, other, tsend.at[0], trecv.at[0], partner)
    swap.start()
    swap.wait()
    attended = part_ref[...].astype(F32) + other[...].astype(F32)
    residual = (tok_ref[...].astype(F32) + attended).astype(BF16)
    ffn = norm_rows(residual.astype(F32), gain_ref[...])
    for s in range(2):
        rows_all[s, i] = ffn[:, s * half : (s + 1) * half]
        resid[s] = residual[:, s * half : (s + 1) * half]

    def gather_copy(slot, dev):
        return remote(
            rows_all.at[t, slot], rows_all.at[t, slot], dsend.at[dev], drecv.at[slot], (dev, t)
        )

    @pl.loop(1, n)
    def _(k):
        gather_copy(i, lax.rem(i + k, n)).start()

    for load in loads[:4]:
        load.wait()
    hidden = (silu(dot(ffn, sg[...])) * dot(ffn, su[...])).astype(BF16)
    sh_send[...] = dot(hidden, sd[u]).astype(BF16)
    shared_swap = remote(sh_send, sh_recv, tsend.at[1], trecv.at[1], partner)
    shared_swap.start()
    sh_keep[...] = dot(hidden, sd[t]).astype(BF16)
    scores = jax.nn.sigmoid(dot_t(router_ref[...], ffn))
    expert_id = lax.broadcasted_iota(jnp.int32, scores.shape, 0)
    routes = routes_ref[...]
    named = routes[0:1] == expert_id
    for k in range(1, routes.shape[0]):
        named = named | (routes[k : k + 1] == expert_id)
    picked = jnp.where(named, scores, 0.0)
    weights[...] = ROUTE_SCALE * picked / jnp.sum(picked, axis=0, keepdims=True)
    diagonal = lax.broadcasted_iota(jnp.int32, (seqs, seqs), 0) == lax.broadcasted_iota(
        jnp.int32, (seqs, seqs), 1
    )
    for load in loads[4:]:
        load.wait()

    def relay(slot):
        return remote(
            rows_all.at[t, slot], rows_all.at[t, slot], rsend.at[slot], rrecv.at[slot], partner
        )

    def relay_in(slot):
        return remote(
            rows_all.at[u, slot], rows_all.at[u, slot], rsend.at[slot], rrecv.at[slot], partner
        )

    def chunk_of(c):
        return lax.rem(i // per_chunk + c, chunks)

    def start_relays(c):
        @pl.loop(0, per_chunk)
        def _(m):
            slot = chunk_of(c) * per_chunk + m

            @pl.when(slot != i)
            def _():
                gather_copy(slot, slot).wait_recv()
                relay(slot).start()

    def part_swap(c):
        return remote(p_send.at[c], p_recv.at[c], psend.at[c], precv.at[c], partner)

    def answer_copy(slot):
        return remote(answer.at[slot], ret.at[i], asend.at[slot], arecv.at[i], (slot, t))

    def finish(c):
        part_swap(c).wait_recv()
        total = (p_keep[c].astype(F32) + p_recv[c].astype(F32)).astype(BF16)
        first = chunk_of(c) * per_chunk
        answer[pl.ds(first, per_chunk)] = total.reshape(per_chunk, seqs, half)

        @pl.loop(0, per_chunk)
        def _(m):
            slot = first + m

            @pl.when(slot != i)
            def _():
                answer_copy(slot).start()

    start_relays(0)

    @pl.loop(0, chunks)
    def _(c):
        @pl.when(c + 1 < chunks)
        def _():
            start_relays(c + 1)

        first = chunk_of(c) * per_chunk

        @pl.loop(0, per_chunk)
        def _(m):
            slot = first + m

            @pl.when(slot != i)
            def _():
                relay_in(slot).wait_recv()

        x0 = rows_all[0, pl.ds(first, per_chunk)].reshape(rows, half)
        x1 = rows_all[1, pl.ds(first, per_chunk)].reshape(rows, half)
        gate = dot(x0, eg[:half]) + dot(x1, eg[half:])
        up = dot(x0, eu[:half]) + dot(x1, eu[half:])
        hid = (silu(gate) * up).astype(BF16)
        p_send[c] = dot(hid, ed[u]).astype(BF16)
        part_swap(c).start()
        p_keep[c] = dot(hid, ed[t]).astype(BF16)

        @pl.when(c > 0)
        def _():
            finish(c - 1)

    finish(chunks - 1)
    shared_swap.wait()
    base = resid[t].astype(F32) + (sh_keep[...].astype(F32) + sh_recv[...].astype(F32))

    def weight_of(e):
        return jnp.sum(jnp.where(diagonal, weights[pl.ds(e, 1), :], 0.0), axis=1, keepdims=True)

    routed = weight_of(i) * answer[i].astype(F32)

    def add(k, acc):
        e = lax.rem(i + k, n)
        remote(answer.at[e], ret.at[e], asend.at[e], arecv.at[e], (e, t)).wait_recv()
        return acc + weight_of(e) * ret[e].astype(F32)

    routed = lax.fori_loop(1, n, add, routed)
    halves[t] = (base + routed).astype(BF16)
    last = remote(halves.at[t], halves.at[t], tsend.at[2], trecv.at[2], partner)
    last.start()

    @pl.loop(1, n)
    def _(k):
        e = lax.rem(i + k, n)
        gather_copy(i, e).wait_send()
        relay(e).wait_send()
        answer_copy(e).wait_send()

    @pl.loop(0, chunks)
    def _(c):
        part_swap(c).wait_send()

    last.wait_send()
    remote(halves.at[u], halves.at[u], tsend.at[2], trecv.at[2], partner).wait_recv()
    for s in range(2):
        out_ref[:, s * half : (s + 1) * half] = halves[s]


def per_device(
    tokens, norm_gain, w_query, w_key, w_value, w_forget, w_out, cache_keys, cache_values,
    cache_gates, lengths, ffn_gain, router_w, routes, shared_gate, shared_up, shared_down,
    expert_gate, expert_up, expert_down,
):
    seqs, width = tokens.shape
    half = width // 2
    n = lax.axis_size("ep")
    positions, kv_width = cache_keys.shape[1:]
    heads = w_forget.shape[1]
    group = heads * HEAD_DIM // kv_width
    per_step = 4

    def whole(a):
        return pl.BlockSpec(a.shape, lambda s: (0,) * a.ndim)

    w_forget = w_forget.T
    partial_value = pl.pallas_call(
        attend_kernel,
        grid=(seqs // per_step,),
        in_specs=[pl.BlockSpec(memory_space=pltpu.SMEM)]
        + [whole(a) for a in (tokens, norm_gain, w_query, w_key, w_value, w_forget, w_out)]
        + [
            pl.BlockSpec((per_step, positions, kv_width), lambda s: (s, 0, 0)),
            pl.BlockSpec((per_step, positions, kv_width), lambda s: (s, 0, 0)),
            pl.BlockSpec((per_step, heads, positions), lambda s: (s, 0, 0)),
        ],
        out_specs=pl.BlockSpec((seqs, width), lambda s: (0, 0)),
        out_shape=jax.ShapeDtypeStruct((seqs, width), BF16),
        scratch_shapes=[
            pltpu.VMEM((seqs, heads, kv_width), F32),
            pltpu.VMEM((seqs, heads, 128), F32),
            pltpu.VMEM((seqs, heads, 128), F32),
            pltpu.VMEM((seqs, kv_width), F32),
            pltpu.VMEM((group, seqs, kv_width), F32),
        ],
        compiler_params=pltpu.CompilerParams(
            dimension_semantics=("arbitrary",)
        ),
        name="attend",
    )(lengths, tokens, norm_gain, w_query, w_key, w_value, w_forget, w_out, cache_keys, cache_values,
      cache_gates)

    per_chunk = 4
    chunks = n // per_chunk
    rows = per_chunk * seqs
    ff = shared_gate.shape[1]
    eff = expert_gate.shape[2]
    vmem = pl.BlockSpec(memory_space=pltpu.VMEM)
    hbm = pl.BlockSpec(memory_space=pl.ANY)
    dma = pltpu.SemaphoreType.DMA
    return pl.pallas_call(
        functools.partial(experts_kernel, n, per_chunk),
        in_specs=[vmem] * 5 + [hbm] * 6,
        out_specs=vmem,
        out_shape=jax.ShapeDtypeStruct((seqs, width), BF16),
        scratch_shapes=[
            pltpu.VMEM((width, ff), BF16),
            pltpu.VMEM((width, ff), BF16),
            pltpu.VMEM((2, ff, half), BF16),
            pltpu.VMEM((width, eff), BF16),
            pltpu.VMEM((width, eff), BF16),
            pltpu.VMEM((2, eff, half), BF16),
            pltpu.VMEM((seqs, width), BF16),
            pltpu.VMEM((2, n, seqs, half), BF16),
            pltpu.VMEM((2, seqs, half), BF16),
            pltpu.VMEM((seqs, half), BF16),
            pltpu.VMEM((seqs, half), BF16),
            pltpu.VMEM((seqs, half), BF16),
            pltpu.VMEM((chunks, rows, half), BF16),
            pltpu.VMEM((chunks, rows, half), BF16),
            pltpu.VMEM((chunks, rows, half), BF16),
            pltpu.VMEM((n, seqs, half), BF16),
            pltpu.VMEM((n, seqs, half), BF16),
            pltpu.VMEM((2, seqs, half), BF16),
            pltpu.VMEM((n, seqs), F32),
            dma((8,)), dma((3,)), dma((3,)),
            dma((n,)), dma((n,)), dma((n,)), dma((n,)),
            dma((chunks,)), dma((chunks,)), dma((n,)), dma((n,)),
        ],
        compiler_params=pltpu.CompilerParams(
            collective_id=0, has_side_effects=True
        ),
        name="experts",
    )(partial_value, tokens, ffn_gain, router_w.T, routes.T, shared_gate, shared_up,
      shared_down, expert_gate, expert_up, expert_down)


def solution(mesh):
    placed = (
        P("ep", None),
        P(),
        P(None, "tp"),
        P(None, "tp"),
        P(None, "tp"),
        P(None, "tp"),
        P("tp", None),
        P("ep", None, "tp"),
        P("ep", None, "tp"),
        P("ep", "tp", None),
        P("ep"),
        P(),
        P(),
        P("ep", None),
        P(None, "tp"),
        P(None, "tp"),
        P("tp", None),
        P("ep", None, "tp"),
        P("ep", None, "tp"),
        P("ep", "tp", None),
    )
    return jax.shard_map(
        per_device, mesh=mesh, in_specs=placed, out_specs=P("ep", None), check_vma=False
    )
```

time: 160 us -> 54 us (0.34); the launches traced: 157 us -> 53.8 us
  waiting for transfers between devices: 81.7 us -> 0 us
  Pallas kernels: 0 us -> 52.3 us
  local copies, waits for them, and re-layouts: 24.5 us -> 1.47 us
  matrix products: 17.9 us -> 0 us
  between operations: 13.8 us -> 0.01 us
  starting transfers between devices: 12.8 us -> 0 us
  other arithmetic: 6.22 us -> 0 us
    pallas_call x0 -> x2, Pallas kernels: none -> 52.3 us  [the longest x1 39 us: per_device(): pl.pallas_call(functools.partial(experts_kernel, n, per_chunk), in_specs=...]
    all_to_all x2 -> x0, waiting for transfers between devices: 41.7 us -> none  [the longest x1 22.1 us: per_device(): lax.all_to_all(merged, 'ep', split_axis=0, concat_axis=0, tiled=True)]
    psum x2 -> x0, waiting for transfers between devices: 39.9 us -> none  [the longest x1 21.2 us: per_device(): merged = lax.psum(part_rows.astype(jnp.bfloat16), 'tp')]
    dot_general x14 -> x0, matrix products: 17.9 us -> none  [the longest x1 3.52 us: attend(): jnp.einsum('skgl,slkd->skgd', past_prob, cached_values, preferred_element...]
    all_to_all x2 -> x0, starting transfers between devices: 12.7 us -> none  [the longest x1 6.36 us: per_device(): lax.all_to_all(merged, 'ep', split_axis=0, concat_axis=0, tiled=True)]
    unnamed x33 -> x1, local copies, waits for them, and re-layouts: 13 us -> 1.47 us
    gather x11 -> x0, local copies, waits for them, and re-layouts: 4.85 us -> none  [the longest x5 2.38 us: attend(): last_gate = jnp.take_along_axis(cache_gates, last_index, axis=2)]
    psum x1 -> x0, local copies, waits for them, and re-layouts: 2.58 us -> none  [per_device(): merged = lax.psum(part_rows.astype(jnp.bfloat16), 'tp')]
  transfers between devices with their start and end apart: 4 -> 0, of which waited for: 4 -> 0; matrix products, arithmetic and copies ran while one was open for 4% -> 0% of each run, Pallas kernels for 0% -> 0%
where the time goes in v1:
time: 54 us; the launch traced here: 53.8 us
  Pallas kernels  52.3 us (97%)
  local copies, waits for them, and re-layouts  1.47 us (3%)
    pallas_call x1, Pallas kernels, per_device(): pl.pallas_call(functools.partial(experts_kernel, n, per_chunk), in_specs=...  39 us
    pallas_call x1, Pallas kernels, per_device(): pl.pallas_call(attend_kernel, grid=(seqs // per_step,), in_specs=[pl.Bloc...  13.3 us
    unnamed x1, local copies, waits for them, and re-layouts  1.47 us

profile of v1, /device:TPU:29, one launch (start us, length us, event | category | flops | bytes accessed | tf_op | source)
XLA Modules:
  0.0 53.8 jit_solution(1259230902948021439)
XLA Ops:
  0.0 13.3 %attend.1.part_ref = bf16[16,2048]{1,0:T(8,128)(2,1)} custom-call(s32[16]{0:T(128)} %len_ref.1, bf16[16,2048]{1,0:T(8,128)(2,1)} %tok_ref.3, bf16[2048]{0:T(1024)(128)(2,1)} %gain_ref.2, bf16[2048,256]{1,0:T(8,128)(2,1)} %wq_ref.1, bf16[2048,128]{1,0:T(8,128)(2,1)} %wk_ref.1, bf16[2048,128]{1,0:T(8,128)(2,1)} %wv_ref.1, bf16[4,2048]{1,0:T(4,128)(2,1)} %bitcast.4, ...), custom_call_target="tpu_custom_call" | custom-call | tf_op jit(solution)/shard_map/attend/pallas_call | solution.py:317
  13.3 39.0 %experts.1 = bf16[16,2048]{1,0:T(8,128)(2,1)} custom-call(bf16[16,2048]{1,0:T(8,128)(2,1)} %attend.1.part_ref, bf16[16,2048]{1,0:T(8,128)(2,1)} %tok_ref.3, bf16[2048]{0:T(1024)(128)(2,1)} %gain_ref.3, bf16[16,2048]{1,0:T(8,128)(2,1)} %bitcast.3, s32[6,16]{1,0:T(8,128)} %bitcast.5, bf16[2048,256]{1,0:T(8,128)(2,1)} %sg_hbm.1, bf16[2048,256]{1,0:T(8,128)(2,1)} %su_hbm.1, ...), custom_call_target="tpu_custom_call" | custom-call | tf_op jit(solution)/shard_map/experts/pallas_call | solution.py:351
  52.3 1.5 %copy.22 = bf16[16,2048]{1,0:T(8,128)(2,1)} copy(bf16[16,2048]{1,0:T(8,128)(2,1)} %experts.1) | data formatting | bytes 131072

commit v2 on v1

--- a/solution.py
+++ b/solution.py
@@ -104,20 +104,23 @@
 
 
 def experts_kernel(
-    n, per_chunk, part_ref, tok_ref, gain_ref, router_ref, routes_ref,
+    n, q, part_ref, tok_ref, gain_ref, router_ref, routes_ref,
     sg_hbm, su_hbm, sd_hbm, eg_hbm, eu_hbm, ed_hbm, out_ref,
     sg, su, sd, eg, eu, ed, other, rows_all, resid, sh_send, sh_recv, sh_keep,
-    p_send, p_recv, p_keep, answer, ret, halves, weights,
-    wsem, tsend, trecv, dsend, drecv, rsend, rrecv, psend, precv, asend, arecv,
+    p_send, p_recv, p_keep, answer, mid, out_sums, in_sums, halves, weights,
+    wsem, tsend, trecv, csend, psend, drecv, rsend, rrecv, xsend, xrecv, asend, arecv,
+    fsend, frecv, vsend, vrecv,
 ):
     i = lax.axis_index("ep")
     t = lax.axis_index("tp")
     u = 1 - t
     seqs, width = tok_ref.shape
     half = width // 2
-    chunks = n // per_chunk
-    rows = per_chunk * seqs
+    planes = n // q
+    rows = q * seqs
     partner = (i, u)
+    zi = i // q
+    pi = lax.rem(i, q)
 
     loads = [
         pltpu.make_async_copy(sg_hbm, sg, wsem.at[0]),
@@ -132,14 +135,23 @@
     for load in loads:
         load.start()
 
+    def plane_of(c):
+        return lax.rem(zi + c, planes)
+
+    def place_of(k):
+        return lax.rem(pi + k, q)
+
     barrier = pltpu.get_barrier_semaphore()
     pl.semaphore_signal(barrier, inc=1, device_id=partner, device_id_type=MESH)
-
-    @pl.loop(1, n)
-    def _(k):
-        pl.semaphore_signal(barrier, inc=1, device_id=(lax.rem(i + k, n), t), device_id_type=MESH)
-
-    pl.semaphore_wait(barrier, n)
+    for c in range(1, planes):
+        pl.semaphore_signal(
+            barrier, inc=1, device_id=(plane_of(c) * q + pi, t), device_id_type=MESH
+        )
+    for k in range(1, q):
+        pl.semaphore_signal(
+            barrier, inc=1, device_id=(zi * q + place_of(k), t), device_id_type=MESH
+        )
+    pl.semaphore_wait(barrier, planes + q - 1)
 
     def remote(src, dst, ssem, rsem, dev):
         return pltpu.make_async_remote_copy(
@@ -157,22 +169,34 @@
         rows_all[s, i] = ffn[:, s * half : (s + 1) * half]
         resid[s] = residual[:, s * half : (s + 1) * half]
 
-    def gather_copy(slot, dev):
+    def landed(dst, rsem):
+        remote(dst, dst, rsend.at[0], rsem, partner).wait_recv()
+
+    def gathered(slot, ssem, dev):
+        return remote(rows_all.at[t, slot], rows_all.at[t, slot], ssem, drecv.at[slot], dev)
+
+    def column_copy(slot, plane):
+        return gathered(slot, csend.at[plane], (plane * q + pi, t))
+
+    def plane_copy(slot, place):
+        return gathered(slot, psend.at[slot // q * q + place], (zi * q + place, t))
+
+    def relay(slot):
         return remote(
-            rows_all.at[t, slot], rows_all.at[t, slot], dsend.at[dev], drecv.at[slot], (dev, t)
-        )
-
-    @pl.loop(1, n)
-    def _(k):
-        gather_copy(i, lax.rem(i + k, n)).start()
-
-    for load in loads[:4]:
-        load.wait()
-    hidden = (silu(dot(ffn, sg[...])) * dot(ffn, su[...])).astype(BF16)
-    sh_send[...] = dot(hidden, sd[u]).astype(BF16)
-    shared_swap = remote(sh_send, sh_recv, tsend.at[1], trecv.at[1], partner)
-    shared_swap.start()
-    sh_keep[...] = dot(hidden, sd[t]).astype(BF16)
+            rows_all.at[t, slot], rows_all.at[t, slot], rsend.at[slot], rrecv.at[slot], partner
+        )
+
+    def relay_in(slot):
+        landed(rows_all.at[u, slot], rrecv.at[slot])
+
+    def spread(slot):
+        for k in range(1, q):
+            plane_copy(slot, place_of(k)).start()
+
+    for c in range(1, planes):
+        column_copy(i, plane_of(c)).start()
+    spread(i)
+
     scores = jax.nn.sigmoid(dot_t(router_ref[...], ffn))
     expert_id = lax.broadcasted_iota(jnp.int32, scores.shape, 0)
     routes = routes_ref[...]
@@ -180,76 +204,65 @@
     for k in range(1, routes.shape[0]):
         named = named | (routes[k : k + 1] == expert_id)
     picked = jnp.where(named, scores, 0.0)
-    weights[...] = ROUTE_SCALE * picked / jnp.sum(picked, axis=0, keepdims=True)
+    weights[zi] = jnp.zeros(weights.shape[1:], F32)
+    weights[zi, :, 0:seqs] = ROUTE_SCALE * picked / jnp.sum(picked, axis=0, keepdims=True)
     diagonal = lax.broadcasted_iota(jnp.int32, (seqs, seqs), 0) == lax.broadcasted_iota(
         jnp.int32, (seqs, seqs), 1
     )
+
+    def weight_copy(src, plane):
+        return remote(
+            weights.at[src], weights.at[src], vsend.at[plane], vrecv.at[src], (plane * q + pi, t)
+        )
+
+    for c in range(1, planes):
+        weight_copy(zi, plane_of(c)).start()
+
+    for load in loads[:4]:
+        load.wait()
+    hidden = (silu(dot(ffn, sg[...])) * dot(ffn, su[...])).astype(BF16)
+    sh_send[...] = dot(hidden, sd[u]).astype(BF16)
+    shared_swap = remote(sh_send, sh_recv, tsend.at[1], trecv.at[1], partner)
+    shared_swap.start()
+
+    def pass_on(c):
+        slot = plane_of(c) * q + pi
+        landed(rows_all.at[t, slot], drecv.at[slot])
+        spread(slot)
+        relay(slot).start()
+
+    for c in range(1, planes):
+        pass_on(c)
+    sh_keep[...] = dot(hidden, sd[t]).astype(BF16)
     for load in loads[4:]:
         load.wait()
 
-    def relay(slot):
+    def start_relays(c):
+        for k in range(1, q):
+            slot = plane_of(c) * q + place_of(k)
+            landed(rows_all.at[t, slot], drecv.at[slot])
+            relay(slot).start()
+
+    def part_swap(c):
+        return remote(p_send.at[c], p_recv.at[c], xsend.at[c], xrecv.at[c], partner)
+
+    def answer_copy(plane, src, place):
         return remote(
-            rows_all.at[t, slot], rows_all.at[t, slot], rsend.at[slot], rrecv.at[slot], partner
-        )
-
-    def relay_in(slot):
+            answer.at[plane * q + place], mid.at[plane * q + src], asend.at[plane * q + place],
+            arecv.at[plane * q + src], (zi * q + place, t),
+        )
+
+    def sum_copy(src, plane):
         return remote(
-            rows_all.at[u, slot], rows_all.at[u, slot], rsend.at[slot], rrecv.at[slot], partner
-        )
-
-    def chunk_of(c):
-        return lax.rem(i // per_chunk + c, chunks)
-
-    def start_relays(c):
-        @pl.loop(0, per_chunk)
-        def _(m):
-            slot = chunk_of(c) * per_chunk + m
-
-            @pl.when(slot != i)
-            def _():
-                gather_copy(slot, slot).wait_recv()
-                relay(slot).start()
-
-    def part_swap(c):
-        return remote(p_send.at[c], p_recv.at[c], psend.at[c], precv.at[c], partner)
-
-    def answer_copy(slot):
-        return remote(answer.at[slot], ret.at[i], asend.at[slot], arecv.at[i], (slot, t))
-
-    def finish(c):
-        part_swap(c).wait_recv()
-        total = (p_keep[c].astype(F32) + p_recv[c].astype(F32)).astype(BF16)
-        first = chunk_of(c) * per_chunk
-        answer[pl.ds(first, per_chunk)] = total.reshape(per_chunk, seqs, half)
-
-        @pl.loop(0, per_chunk)
-        def _(m):
-            slot = first + m
-
-            @pl.when(slot != i)
-            def _():
-                answer_copy(slot).start()
-
-    start_relays(0)
-
-    @pl.loop(0, chunks)
-    def _(c):
-        @pl.when(c + 1 < chunks)
-        def _():
-            start_relays(c + 1)
-
-        first = chunk_of(c) * per_chunk
-
-        @pl.loop(0, per_chunk)
-        def _(m):
-            slot = first + m
-
-            @pl.when(slot != i)
-            def _():
-                relay_in(slot).wait_recv()
-
-        x0 = rows_all[0, pl.ds(first, per_chunk)].reshape(rows, half)
-        x1 = rows_all[1, pl.ds(first, per_chunk)].reshape(rows, half)
+            out_sums.at[plane], in_sums.at[src], fsend.at[plane], frecv.at[src], (plane * q + pi, t)
+        )
+
+    def compute(c):
+        first = plane_of(c) * q
+        for k in range(1 if isinstance(c, int) and c == 0 else 0, q):
+            relay_in(first + place_of(k))
+        x0 = rows_all[0, pl.ds(first, q)].reshape(rows, half)
+        x1 = rows_all[1, pl.ds(first, q)].reshape(rows, half)
         gate = dot(x0, eg[:half]) + dot(x1, eg[half:])
         up = dot(x0, eu[:half]) + dot(x1, eu[half:])
         hid = (silu(gate) * up).astype(BF16)
@@ -257,42 +270,84 @@
         part_swap(c).start()
         p_keep[c] = dot(hid, ed[t]).astype(BF16)
 
-        @pl.when(c > 0)
+    def finish(c):
+        part_swap(c).wait_recv()
+        total = (p_keep[c].astype(F32) + p_recv[c].astype(F32)).astype(BF16)
+        plane = plane_of(c)
+        answer[pl.ds(plane * q, q)] = total.reshape(q, seqs, half)
+        for k in range(1, q):
+            answer_copy(plane, pi, place_of(k)).start()
+
+    def plane_sum(c):
+        plane = plane_of(c)
+        if not (isinstance(c, int) and c == 0):
+            landed(weights.at[plane], vrecv.at[plane])
+        total = jnp.zeros((seqs, half), F32)
+        for k in range(q):
+            place = place_of(k)
+            if k:
+                landed(mid.at[plane * q + place], arecv.at[plane * q + place])
+                block = mid[plane * q + place]
+            else:
+                block = answer[plane * q + pi]
+            row = weights[plane, pl.ds(zi * q + place, 1), 0:seqs]
+            column = jnp.sum(jnp.where(diagonal, row, 0.0), axis=1, keepdims=True)
+            total = total + column * block.astype(F32)
+        if isinstance(c, int) and c == 0:
+            return total
+        out_sums[plane] = total.astype(BF16)
+        sum_copy(zi, plane).start()
+
+    start_relays(0)
+    if planes > 1:
+        start_relays(1)
+    compute(0)
+
+    @pl.loop(1, planes)
+    def _(c):
+        @pl.when(c + 1 < planes)
         def _():
-            finish(c - 1)
-
-    finish(chunks - 1)
+            start_relays(c + 1)
+
+        compute(c)
+        finish(c - 1)
+
+        @pl.when(c > 2)
+        def _():
+            plane_sum(c - 2)
+
+    finish(planes - 1)
     shared_swap.wait()
-    base = resid[t].astype(F32) + (sh_keep[...].astype(F32) + sh_recv[...].astype(F32))
-
-    def weight_of(e):
-        return jnp.sum(jnp.where(diagonal, weights[pl.ds(e, 1), :], 0.0), axis=1, keepdims=True)
-
-    routed = weight_of(i) * answer[i].astype(F32)
-
-    def add(k, acc):
-        e = lax.rem(i + k, n)
-        remote(answer.at[e], ret.at[e], asend.at[e], arecv.at[e], (e, t)).wait_recv()
-        return acc + weight_of(e) * ret[e].astype(F32)
-
-    routed = lax.fori_loop(1, n, add, routed)
-    halves[t] = (base + routed).astype(BF16)
+    routed = plane_sum(0)
+    for c in range(max(1, planes - 2), planes):
+        plane_sum(c)
+    routed = routed + (
+        resid[t].astype(F32) + (sh_keep[...].astype(F32) + sh_recv[...].astype(F32))
+    )
+    for c in range(1, planes):
+        plane = plane_of(c)
+        landed(in_sums.at[plane], frecv.at[plane])
+        routed = routed + in_sums[plane].astype(F32)
+    halves[t] = routed.astype(BF16)
     last = remote(halves.at[t], halves.at[t], tsend.at[2], trecv.at[2], partner)
     last.start()
 
-    @pl.loop(1, n)
-    def _(k):
-        e = lax.rem(i + k, n)
-        gather_copy(i, e).wait_send()
-        relay(e).wait_send()
-        answer_copy(e).wait_send()
-
-    @pl.loop(0, chunks)
-    def _(c):
+    for c in range(planes):
+        plane = plane_of(c)
         part_swap(c).wait_send()
+        if c:
+            column_copy(i, plane).wait_send()
+            weight_copy(zi, plane).wait_send()
+            sum_copy(zi, plane).wait_send()
+        for k in range(q):
+            if k:
+                plane_copy(plane * q + pi, place_of(k)).wait_send()
+                answer_copy(plane, pi, place_of(k)).wait_send()
+            if c or k:
+                relay(plane * q + place_of(k)).wait_send()
 
     last.wait_send()
-    remote(halves.at[u], halves.at[u], tsend.at[2], trecv.at[2], partner).wait_recv()
+    landed(halves.at[u], trecv.at[2])
     for s in range(2):
         out_ref[:, s * half : (s + 1) * half] = halves[s]
 
@@ -371,11 +426,14 @@
             pltpu.VMEM((chunks, rows, half), BF16),
             pltpu.VMEM((n, seqs, half), BF16),
             pltpu.VMEM((n, seqs, half), BF16),
+            pltpu.VMEM((chunks, seqs, half), BF16),
+            pltpu.VMEM((chunks, seqs, half), BF16),
             pltpu.VMEM((2, seqs, half), BF16),
-            pltpu.VMEM((n, seqs), F32),
+            pltpu.VMEM((chunks, n, 128), F32),
             dma((8,)), dma((3,)), dma((3,)),
-            dma((n,)), dma((n,)), dma((n,)), dma((n,)),
+            dma((chunks,)), dma((n,)), dma((n,)), dma((n,)), dma((n,)),
             dma((chunks,)), dma((chunks,)), dma((n,)), dma((n,)),
+            dma((chunks,)), dma((chunks,)), dma((chunks,)), dma((chunks,)),
         ],
         compiler_params=pltpu.CompilerParams(
             collective_id=0, has_side_effects=True

time: 54 us -> 48.5 us (0.90)
  the two profiles are of different devices: /device:TPU:29 before, /device:TPU:0 now
where the time goes in v2:
time: 48.5 us; the launch traced here: 48.3 us
  Pallas kernels  46.8 us (96%)
  local copies, waits for them, and re-layouts  1.47 us (3%)
    pallas_call x1, Pallas kernels, per_device(): pl.pallas_call(functools.partial(experts_kernel, n, per_chunk), in_specs=...  33.5 us
    pallas_call x1, Pallas kernels, per_device(): pl.pallas_call(attend_kernel, grid=(seqs // per_step,), in_specs=[pl.Bloc...  13.3 us
    unnamed x1, local copies, waits for them, and re-layouts  1.47 us

profile of v2, /device:TPU:0, one launch (start us, length us, event | category | flops | bytes accessed | tf_op | source)
XLA Modules:
  0.0 48.3 jit_solution(8932358214887825207)
XLA Ops:
  0.0 13.3 %attend.1.part_ref = bf16[16,2048]{1,0:T(8,128)(2,1)} custom-call(s32[16]{0:T(128)} %len_ref.1, bf16[16,2048]{1,0:T(8,128)(2,1)} %tok_ref.3, bf16[2048]{0:T(1024)(128)(2,1)} %gain_ref.2, bf16[2048,256]{1,0:T(8,128)(2,1)} %wq_ref.1, bf16[2048,128]{1,0:T(8,128)(2,1)} %wk_ref.1, bf16[2048,128]{1,0:T(8,128)(2,1)} %wv_ref.1, bf16[4,2048]{1,0:T(4,128)(2,1)} %bitcast.4, ...), custom_call_target="tpu_custom_call" | custom-call | tf_op jit(solution)/shard_map/attend/pallas_call | solution.py:372
  13.3 33.5 %experts.1 = bf16[16,2048]{1,0:T(8,128)(2,1)} custom-call(bf16[16,2048]{1,0:T(8,128)(2,1)} %attend.1.part_ref, bf16[16,2048]{1,0:T(8,128)(2,1)} %tok_ref.3, bf16[2048]{0:T(1024)(128)(2,1)} %gain_ref.3, bf16[16,2048]{1,0:T(8,128)(2,1)} %bitcast.3, s32[6,16]{1,0:T(8,128)} %bitcast.5, bf16[2048,256]{1,0:T(8,128)(2,1)} %sg_hbm.1, bf16[2048,256]{1,0:T(8,128)(2,1)} %su_hbm.1, ...), custom_call_target="tpu_custom_call" | custom-call | tf_op jit(solution)/shard_map/experts/pallas_call | solution.py:406
  46.8 1.5 %copy.22 = bf16[16,2048]{1,0:T(8,128)(2,1)} copy(bf16[16,2048]{1,0:T(8,128)(2,1)} %experts.1) | data formatting | bytes 131072
